TPU v7x, 128 devices: a whole 4x4x4 slice. The times are simulated.
128 devices in a mesh: sp: 16 (over z, y), tp: 8 (over x, core).
Axes of the slice: x: 4, y: 4, z: 4, core: 2. Of those that a mesh axis runs over, the one named last changes fastest.
Arguments:
- inputs: bfloat16 [16384, 4, 2048], P('sp'), may hold values from -6 to 6
- norm_gain: float32 [2048], replicated, may hold values from 0.1 to 1.9
- pool_proj: bfloat16 [2048, 1024], P(None, 'tp'), may hold values from -0.125 to 0.125
- pool_gate_proj: bfloat16 [2048, 1024], P(None, 'tp'), may hold values from -0.125 to 0.125
- pool_mix: bfloat16 [8, 128, 128], P('tp'), may hold values from -0.5 to 0.5
- query_proj: bfloat16 [2048, 1024], P(None, 'tp'), may hold values from -0.125 to 0.125
- key_proj: bfloat16 [2048, 512], P(None, 'tp'), may hold values from -0.125 to 0.125
- value_proj: bfloat16 [2048, 512], P(None, 'tp'), may hold values from -0.125 to 0.125
- attn_gate_proj: bfloat16 [2048, 1024], P(None, 'tp'), may hold values from -0.125 to 0.125
- query_gain: float32 [64], replicated, may hold values from 0.1 to 1.9
- key_gain: float32 [64], replicated, may hold values from 0.1 to 1.9
- sink_logit: float32 [16], P('tp'), may hold values from -12 to 240
- out_pool: bfloat16 [1024, 2048], P('sp'), may hold values from -0.125 to 0.125
- out_attn: bfloat16 [1024, 2048], P('sp'), may hold values from -0.125 to 0.125
Outputs:
- mixed_out: bfloat16 [16384, 4, 2048], P(('sp', 'tp'))
- log_weight_sum: float32 [16384, 4, 16], P('sp', None, 'tp')
All inputs are finite; a program needn't handle non-finite values.
Results may differ from a plain program's by a relative error of at most 0.015.
Values may be sent and summed in bfloat16 or wider, within the bound.
A program may use at most 192 MiB of HBM per device.

v0:
```python
import functools

import jax
import jax.numpy as jnp
from jax import lax
from jax.experimental import pallas as pl
from jax.experimental.pallas import tpu as pltpu
from jax.sharding import PartitionSpec as P

HEADS = 16
EPS = 1e-06
NEG = -1e30
SHIFT = 29.5
LOG2E = 1.4426950408889634
BF = jnp.bfloat16
F32 = jnp.float32
SEQ_LEN = 16384
NSP = 16
COMM = True


def split_dot(values, ones):
    hi = values.astype(BF)
    lo = (values - hi.astype(F32)).astype(BF)
    return jnp.dot(hi, ones, preferred_element_type=F32) + jnp.dot(lo, ones, preferred_element_type=F32)


def silu(v):
    return v / (1.0 + jnp.exp(-v))


def kernel(
    x_hbm, gain, pw, gw, qw, kw, vw, aw, mix, qg, kg, sink, outp, outa,
    out, lse,
    xb, wb, kst, vst, tmp, qs, kvs, poolbuf, gate, agate, bias, band, ysend, yr, wg, acc, att, lseb,
    xsem, wsem, asend, arecv, hsend, hrecv, gsend, grecv, dsend, drecv,
):
    if COMM:
        sp = lax.axis_index("sp")
        tp = lax.axis_index("tp")
    else:
        sp = jnp.int32(0)
        tp = jnp.int32(0)
    chip = tp // 2
    c = tp % 2
    y = sp % 4
    z = sp // 4
    a = y * (1 - c) + z * c
    b_ = z * (1 - c) + y * c
    sa = 1 + 3 * c
    sb = 4 - 3 * c

    def order(k):
        return (2 * chip + 1 - c + k - 2 * c * k + 16) % 8

    def xcopy(k):
        return pltpu.make_async_copy(
            x_hbm.at[pl.ds(order(k) * 128, 128)], xb.at[k % 2], xsem.at[k % 2]
        )

    wcopies = [
        pltpu.make_async_copy(outp, wg.at[0, sp], wsem.at[0]),
        pltpu.make_async_copy(outa, wg.at[1, sp], wsem.at[1]),
        pltpu.make_async_copy(pw, wb.at[:, pl.ds(0, 128)], wsem.at[2]),
        pltpu.make_async_copy(gw, wb.at[:, pl.ds(128, 128)], wsem.at[3]),
        pltpu.make_async_copy(qw, wb.at[:, pl.ds(256, 128)], wsem.at[4]),
        pltpu.make_async_copy(kw, kst, wsem.at[5]),
        pltpu.make_async_copy(vw, vst, wsem.at[6]),
        pltpu.make_async_copy(aw, wb.at[:, pl.ds(512, 128)], wsem.at[7]),
    ]
    for cp in wcopies:
        cp.start()
    xcopy(0).start()
    xcopy(1).start()

    zeros = jnp.zeros((64, 128), BF)
    poolbuf[0:64, :] = zeros
    poolbuf[64 + 4096 : 128 + 4096, :] = zeros
    for s in range(4):
        kvs[s, 0:128, :] = jnp.zeros((128, 128), BF)
        kvs[s, 9 * 128 : 10 * 128, :] = jnp.zeros((128, 128), BF)

    def remote(src, dst, ss, rs, dev):
        return pltpu.make_async_remote_copy(
            src_ref=src, dst_ref=dst, send_sem=ss, recv_sem=rs,
            device_id=dev, device_id_type=pl.DeviceIdType.MESH,
        )

    if COMM:
        barrier = pltpu.get_barrier_semaphore()

        def greet(dev):
            pl.semaphore_signal(barrier, inc=1, device_id=dev, device_id_type=pl.DeviceIdType.MESH)

        for j in range(1, 8):
            greet((sp, (tp + j) % 8))
        greet((z * 4 + (y + 1) % 4, tp))
        greet((z * 4 + (y + 3) % 4, tp))
        greet((((z + 1) % 4) * 4 + y, tp))
        greet((((z + 3) % 4) * 4 + y, tp))

        greet(((sp + 1) % NSP, tp))
        greet(((sp + NSP - 1) % NSP, tp))
        pl.semaphore_wait(barrier, 13)

    def slice_at(da, db):
        return ((a + da) % 4) * sa + ((b_ + db) % 4) * sb

    def piece(da, db, half):
        if half is None:
            return wg.at[c, slice_at(da, db)]
        return wg.at[c, slice_at(da, db), pl.ds(32 * half, 32)]

    sends = []

    def gcopy(da, db, half, ma, mb, n):
        return remote(
            piece(da, db, half), piece(da, db, half), gsend.at[n],
            grecv.at[((da - ma) % 4) * 4 + (db - mb) % 4, half or 0],
            (slice_at(ma, mb), tp),
        )

    def send(da, db, half, ma, mb):
        if COMM:
            n = len(sends)
            sends.append((da, db, half, ma, mb, n))
            gcopy(da, db, half, ma, mb, n).start()

    def got(da, db, half=None):
        if COMM:
            ref = piece(da, db, half)
            remote(
                ref, ref, gsend.at[0], grecv.at[da * 4 + db, half or 0], (sp, tp + 1 - 2 * c)
            ).wait_recv()

    def across(da, db):
        ref = piece(da, db, None)
        return remote(
            ref, ref, dsend.at[da * 4 + db], drecv.at[da * 4 + db], (sp, tp + 1 - 2 * c)
        )

    def share(da, db):
        if COMM:
            across(da, db).start()

    def event0():
        send(0, 0, None, 1, 0)
        send(0, 0, None, -1, 0)
        send(0, 0, None, 0, 1)
        send(0, 0, None, 0, -1)

    def event1():
        got(3, 0)
        send(3, 0, 0, 1, 0)
        got(1, 0)
        send(1, 0, 1, -1, 0)
        for da in (3, 1):
            send(da, 0, None, 0, 1)
            send(da, 0, None, 0, -1)
            share(da, 0)

    def through(da):
        got(da, 3)
        send(da, 3, 0, 0, 1)
        share(da, 3)
        got(da, 1)
        send(da, 1, 1, 0, -1)
        share(da, 1)

    def far(da):
        got(da, 2, 0)
        got(da, 2, 1)
        share(da, 2)

    def event2():
        got(2, 0, 0)
        got(2, 0, 1)
        send(2, 0, None, 0, 1)
        send(2, 0, None, 0, -1)
        share(2, 0)
        through(0)

    def event3():
        through(3)
        through(1)
        far(0)

    def event4():
        through(2)
        far(3)
        far(1)

    def event5():
        far(2)

    wcopies[0].wait()
    wcopies[1].wait()
    event0()

    lane = lax.broadcasted_iota(jnp.int32, (1, 128), 1)
    low = lane < 64
    ones = jnp.ones((128, 128), BF)
    head_ones = (
        (lax.broadcasted_iota(jnp.int32, (128, 128), 0) // 64)
        == (lax.broadcasted_iota(jnp.int32, (128, 128), 1) // 64)
    ).astype(F32).astype(BF)

    tpf = tp.astype(F32)
    s0 = sink[0]
    s1 = sink[1]
    m0 = jnp.maximum(s0, SHIFT)
    m1 = jnp.maximum(s1, SHIFT)
    for h in range(2):
        slope = jnp.exp2(jnp.full((128, 128), -(2.0 * tpf + (h + 1.0)) * 0.5, F32))
        m = (m0, m1)[h]
        for p in range(3):
            i = lax.broadcasted_iota(jnp.int32, (128, 128), 0)
            j = lax.broadcasted_iota(jnp.int32, (128, 128), 1)
            dist = jnp.abs(i - j - (128 * p - 128))
            val = (-slope * dist.astype(F32) - m) * LOG2E
            bias[p, 128 * h : 128 * h + 128, :] = jnp.where(dist <= 128, val, NEG)
        bias[3, 128 * h : 128 * h + 128, :] = jnp.full((128, 128), NEG, F32)

    hw = jnp.left_shift(jnp.int32(1), tp % 4)
    delta = (
        lax.broadcasted_iota(jnp.int32, (128, 256), 1)
        - 64
        - lax.broadcasted_iota(jnp.int32, (128, 256), 0)
    )
    band[...] = (
        ((delta + 1024) % 4 == 0) & (delta >= -4 * hw) & (delta <= 4 * hw - 4)
    ).astype(F32).astype(BF)

    for cp in wcopies[2:]:
        cp.wait()

    def prep(l, carry):
        rows = pl.ds(pl.multiple_of(l * 128, 128), 128)
        g = jnp.transpose(jnp.broadcast_to(gain[pl.ds(l, 1), :], (128, 128)))
        for t in (0, 1, 2, 4):
            cols = slice(128 * t, 128 * t + 128)
            wb[rows, cols] = (wb[rows, cols].astype(F32) * g).astype(BF)
        kv = jnp.concatenate([kst[rows, :].astype(F32), vst[rows, :].astype(F32)], axis=1)
        wb[rows, 384:512] = (kv * g).astype(BF)
        return carry

    lax.fori_loop(0, 16, prep, 0)

    qgain = jnp.concatenate([qg[...], qg[...]], axis=1) * (0.125 * LOG2E)
    kgain = jnp.concatenate([kg[...], kg[...]], axis=1)

    def halo(i, src, dst, dev):
        return remote(src, dst, hsend.at[i], hrecv.at[i], dev)

    def halo_left():
        return (
            halo(0, kvs.at[:, pl.ds(128, 128), :], kvs.at[:, pl.ds(9 * 128, 128), :], (sp - 1, tp)),
            halo(1, poolbuf.at[pl.ds(64, 32)], poolbuf.at[pl.ds(64 + 4096, 32)], (sp - 1, tp)),
        )

    def halo_right():
        return (
            halo(2, kvs.at[:, pl.ds(8 * 128, 128), :], kvs.at[:, pl.ds(0, 128), :], (sp + 1, tp)),
            halo(3, poolbuf.at[pl.ds(64 + 4096 - 32, 32)], poolbuf.at[pl.ds(32, 32)], (sp + 1, tp)),
        )

    def project(k, blk):
        xcopy(k).wait()
        x = xb[k % 2].reshape(512, 2048)
        sq = jnp.zeros((512, 128), F32)
        for l in range(16):
            t = x[:, 128 * l : 128 * l + 128].astype(F32)
            sq = sq + t * t
        r = lax.rsqrt(split_dot(sq, ones) * (1.0 / 2048) + EPS)
        p = jnp.dot(x, wb[...], preferred_element_type=F32)
        rows = pl.ds(pl.multiple_of(blk * 512, 512), 512)
        prows = pl.ds(pl.multiple_of(blk * 512 + 64, 64), 512)
        poolbuf[prows, :] = (p[:, 0:128] * r).astype(BF)
        gate[rows, :] = (p[:, 128:256] * r).astype(BF)
        agate[rows, :] = (p[:, 512:640] * r).astype(BF)
        q = (p[:, 256:384] * r).astype(BF).astype(F32)
        rq = lax.rsqrt(split_dot(q * q, head_ones) * (1.0 / 64) + EPS)
        tmp[0] = q * rq * qgain
        kv = (p[:, 384:512] * r).astype(BF).astype(F32)
        rk = lax.rsqrt(split_dot(kv * kv, head_ones) * (1.0 / 64) + EPS)
        tmp[1] = jnp.where(low, kv * rk * kgain, kv)
        for s in range(4):
            q = tmp[0, pl.ds(s, 128, stride=4), :]
            qs[blk, s, 0:128, :] = jnp.where(low, q, 0.0).astype(BF)
            qs[blk, s, 128:256, :] = jnp.where(low, pltpu.roll(q, 64, 1), 0.0).astype(BF)
            kvs[s, pl.ds(pl.multiple_of((blk + 1) * 128, 128), 128), :] = tmp[
                1, pl.ds(s, 128, stride=4), :
            ].astype(BF)

        @pl.when(k + 2 < 8)
        def _():
            xcopy(k + 2).start()

        if COMM:
            @pl.when((blk == 0) & (sp > 0))
            def _():
                for cp in halo_left():
                    cp.start()

            @pl.when((blk == 7) & (sp < NSP - 1))
            def _():
                for cp in halo_right():
                    cp.start()

    def emit(part, blk, value):
        @pl.when(blk == tp)
        def _():
            yr[part, blk] = value

        @pl.when(blk != tp)
        def _():
            ysend[part, blk] = value
            if COMM:
                remote(
                    ysend.at[part, blk], yr.at[part, tp], asend.at[part, blk], arecv.at[part, tp], (sp, blk)
                ).start()

    def pool(blk):
        if COMM:
            @pl.when((blk == 0) & (sp > 0))
            def _():
                halo_right()[1].wait_recv()

            @pl.when((blk == 7) & (sp < NSP - 1))
            def _():
                halo_left()[1].wait_recv()

        start = pl.multiple_of(blk * 512, 512)
        sums = jnp.concatenate(
            [
                jnp.dot(band[...], poolbuf[pl.ds(start + 128 * g, 256), :], preferred_element_type=F32)
                for g in range(4)
            ],
            axis=0,
        )
        pos = sp * 1024 + blk * 128 + lax.broadcasted_iota(jnp.int32, (512, 128), 0) // 4
        lo = jnp.maximum(pos - hw, 0)
        hi = jnp.minimum(pos + hw - 1, SEQ_LEN - 1)
        count = (hi - lo + 1).astype(F32)
        own = poolbuf[pl.ds(start + 64, 512), :].astype(F32)
        pooled = (sums / count - own).astype(BF)
        mixed = jnp.dot(pooled, mix[0], preferred_element_type=F32)
        g = gate[pl.ds(start, 512), :].astype(F32)
        emit(0, blk, (mixed * silu(g)).astype(BF))

    def proj_step(k, carry):
        project(k, order(k))

        @pl.when(k >= 3)
        def _():
            pool(order(k - 2))

        if COMM:
            for at, event in ((2, event1), (4, event2), (6, event3)):
                pl.when(k == at)(event)
        return carry

    lax.fori_loop(0, 8, proj_step, 0)

    def pool_rest(k, carry):
        pool(order(k % 8))
        return carry

    lax.fori_loop(6, 9, pool_rest, 0)

    sp0 = 1 - (sp + 15) // 16
    sp15 = (sp + 1) // 16

    def attend(blk):
        if COMM:
            @pl.when((blk == 0) & (sp > 0))
            def _():
                halo_right()[0].wait_recv()

            @pl.when((blk == 7) & (sp < NSP - 1))
            def _():
                halo_left()[0].wait_recv()

        left = 3 * sp0 * (1 - (blk + 7) // 8)
        right = 2 + sp15 * ((blk + 1) // 8)
        for s in range(4):
            q = qs[blk, s]
            kv = kvs[s, pl.ds(pl.multiple_of(blk * 128, 128), 384), :]
            scores = lax.dot_general(q, kv, (((1,), (1,)), ((), ())), preferred_element_type=F32)
            w = jnp.concatenate(
                [
                    jnp.exp2(scores[:, 128 * p : 128 * p + 128] + bias[at]).astype(BF)
                    for p, at in ((0, left), (1, 1), (2, right))
                ],
                axis=1,
            )
            rhs = jnp.concatenate([kv, jnp.ones((384, 128), BF)], axis=1)
            o = jnp.dot(w, rhs, preferred_element_type=F32)
            t0 = o[0:128, 128:256] + jnp.exp(jnp.full((128, 128), s0 - m0, F32))
            t1 = o[128:256, 128:256] + jnp.exp(jnp.full((128, 128), s1 - m1, F32))
            both = jnp.where(
                low, pltpu.roll(o[0:128, 0:128], 64, 1) / t0, o[128:256, 0:128] / t1
            )
            att[pl.ds(s, 128, stride=4), :] = both
            lseb[pl.ds(s, 128, stride=4), :] = jnp.where(
                lane == 0, m0 + jnp.log(t0), m1 + jnp.log(t1)
            )
        g = agate[pl.ds(pl.multiple_of(blk * 512, 512), 512), :].astype(F32)
        emit(1, blk, (att[...] * silu(g)).astype(BF))
        lse[pl.ds(pl.multiple_of(blk * 128, 128), 128)] = lseb[:, 0:2].reshape(128, 4, 2)

    def att_step(k, carry):
        j = k // 2
        d = (2 + 3 * j + 3 * (j // 2) + 2 * (j // 3)) % 4
        d = (d + c * (4 - 2 * d)) % 4
        attend(((chip + d) % 4) * 2 + (c + 1 + k) % 2)
        if COMM:
            for at, event in ((1, event4), (5, event5)):
                pl.when(k == at)(event)
        return carry

    lax.fori_loop(0, 8, att_step, 0)

    def exchange(part, j):
        return remote(
            ysend.at[part, j], yr.at[part, tp], asend.at[part, j], arecv.at[part, j], (sp, j)
        )

    def arrive(part):
        if COMM:
            for j in range(8):
                @pl.when(tp != j)
                def _():
                    remote(
                        ysend.at[part, j], yr.at[part, j], asend.at[part, j], arecv.at[part, j], (sp, j)
                    ).wait_recv()

    if COMM:
        for da in range(4):
            for db in range(4):
                if da or db:
                    ref = wg.at[1 - c, ((b_ + da) % 4) * sb + ((a + db) % 4) * sa]
                    remote(
                        ref, ref, dsend.at[da * 4 + db], drecv.at[da * 4 + db], (sp, tp + 1 - 2 * c)
                    ).wait_recv()

    arrive(0)

    def out_pool_step(n, carry):
        cols = pl.ds(pl.multiple_of(n * 256, 256), 256)
        acts = jnp.concatenate([yr[0, j] for j in range(8)], axis=1)
        acc[:, cols] = jnp.dot(
            acts, wg[0, :, :, cols].reshape(1024, 256), preferred_element_type=F32
        )
        return carry

    lax.fori_loop(0, 8, out_pool_step, 0)
    arrive(1)

    def out_attn_step(n, carry):
        cols = pl.ds(pl.multiple_of(n * 256, 256), 256)
        acts = jnp.concatenate([yr[1, j] for j in range(8)], axis=1)
        total = acc[:, cols] + jnp.dot(
            acts, wg[1, :, :, cols].reshape(1024, 256), preferred_element_type=F32
        )
        out[:, :, cols] = total.astype(BF).reshape(128, 4, 256)
        return carry

    lax.fori_loop(0, 8, out_attn_step, 0)

    if COMM:
        for part in range(2):
            for j in range(8):
                @pl.when(tp != j)
                def _():
                    exchange(part, j).wait_send()
        for item in sends:
            gcopy(*item).wait_send()
        for da in range(4):
            for db in range(4):
                if da or db:
                    across(da, db).wait_send()

        @pl.when(sp > 0)
        def _():
            for cp in halo_left():
                cp.wait_send()

        @pl.when(sp < NSP - 1)
        def _():
            for cp in halo_right():
                cp.wait_send()


def layer(
    inputs, norm_gain, pool_proj, pool_gate_proj, pool_mix, query_proj, key_proj, value_proj,
    attn_gate_proj, query_gain, key_gain, sink_logit, out_pool, out_attn,
):
    hbm = pl.BlockSpec(memory_space=pl.ANY)
    vmem = pl.BlockSpec(memory_space=pltpu.VMEM)
    smem = pl.BlockSpec(memory_space=pltpu.SMEM)
    dma = pltpu.SemaphoreType.DMA
    return pl.pallas_call(
        kernel,
        out_shape=(
            jax.ShapeDtypeStruct((128, 4, 2048), BF),
            jax.ShapeDtypeStruct((1024, 4, 2), F32),
        ),
        in_specs=[hbm, vmem, hbm, hbm, hbm, hbm, hbm, hbm, vmem, vmem, vmem, smem, hbm, hbm],
        out_specs=(vmem, vmem),
        scratch_shapes=[
            pltpu.VMEM((2, 128, 4, 2048), BF),
            pltpu.VMEM((2048, 640), BF),
            pltpu.VMEM((2048, 64), BF),
            pltpu.VMEM((2048, 64), BF),
            pltpu.VMEM((2, 512, 128), F32),
            pltpu.VMEM((8, 4, 256, 128), BF),
            pltpu.VMEM((4, 1280, 128), BF),
            pltpu.VMEM((4096 + 128, 128), BF),
            pltpu.VMEM((4096, 128), BF),
            pltpu.VMEM((4096, 128), BF),
            pltpu.VMEM((4, 256, 128), F32),
            pltpu.VMEM((128, 256), BF),
            pltpu.VMEM((2, 8, 512, 128), BF),
            pltpu.VMEM((2, 8, 512, 128), BF),
            pltpu.VMEM((2, 16, 64, 2048), BF),
            pltpu.VMEM((512, 2048), F32),
            pltpu.VMEM((512, 128), F32),
            pltpu.VMEM((512, 128), F32),
            dma((2,)), dma((8,)),
            dma((2, 8)), dma((2, 8)),
            dma((4,)), dma((4,)),
            dma((24,)), dma((16, 2)),
            dma((16,)), dma((16,)),
        ],
        compiler_params=pltpu.CompilerParams(
            vmem_limit_bytes=60 * 1024 * 1024,
            **(dict(collective_id=0, has_side_effects=True) if COMM else {}),
        ),
        name="mixer_layer",
    )(
        inputs, norm_gain.reshape(16, 128), pool_proj, pool_gate_proj, query_proj, key_proj,
        value_proj, attn_gate_proj, pool_mix, query_gain.reshape(1, 64), key_gain.reshape(1, 64),
        sink_logit, out_pool, out_attn,
    )


def solution(mesh):
    placed = (
        P("sp", None, None), P(), P(None, "tp"), P(None, "tp"), P("tp", None, None), P(None, "tp"),
        P(None, "tp"), P(None, "tp"), P(None, "tp"), P(), P(), P("tp"), P("sp", None), P("sp", None),
    )
    return jax.shard_map(
        layer,
        mesh=mesh,
        in_specs=placed,
        out_specs=(P(("sp", "tp"), None, None), P("sp", None, "tp")),
        check_vma=False,
    )
```

profile of v0, /device:TPU:33, one launch (start us, length us, event | category | flops | bytes accessed | tf_op | source)
XLA Modules:
  0.0 71.0 jit_solution(5169774515945756865)
XLA Ops:
  0.6 2.0 %copy.16.kw = bf16[2048,64]{1,0:T(8,128)(2,1)} copy(bf16[2048,64]{0,1:T(8,128)(2,1)} %param.20) | data formatting | bytes 524288 | tf_op args[6]
  2.6 2.0 %copy.17.vw = bf16[2048,64]{1,0:T(8,128)(2,1)} copy(bf16[2048,64]{0,1:T(8,128)(2,1)} %param.21) | data formatting | bytes 524288 | tf_op args[7]
  4.5 62.5 %mixer_layer.1 = (bf16[128,4,2048]{2,1,0:T(4,128)(2,1)}, f32[1024,4,2]{2,1,0:T(4,128)}) custom-call(bf16[1024,4,2048]{2,1,0:T(4,128)(2,1)} %x_hbm.1, f32[16,128]{1,0:T(8,128)} %bitcast.3, bf16[2048,128]{1,0:T(8,128)(2,1)} %pw.1, bf16[2048,128]{1,0:T(8,128)(2,1)} %gw.1, bf16[2048,128]{1,0:T(8,128)(2,1)} %qw.1, bf16[2048,64]{1,0:T(8,128)(2,1)} %copy.16.kw, ...), custom_call_target="tpu_custom_call" | custom-call | tf_op jit(solution)/shard_map/mixer_layer/pallas_call | solution.py:503
  67.0 0.0 copy-start
  67.0 2.6 %copy.18 = f32[1024,4,2]{0,2,1:T(2,128)} copy(f32[1024,4,2]{2,1,0:T(4,128)} %get-tuple-element.3) | data formatting | bytes 65536 | tf_op jit(solution)/shard_map/mixer_layer/pallas_call | solution.py:503
  69.7 0.0 copy-done
  69.7 1.3 %copy.20 = bf16[128,4,2048]{2,1,0:T(4,128)(2,1)} copy(bf16[128,4,2048]{2,1,0:T(4,128)(2,1)S(1)} %copy-done) | data formatting | bytes 4194304
Async XLA Ops:
  67.0 2.7 %copy-start = (bf16[128,4,2048]{2,1,0:T(4,128)(2,1)S(1)}, bf16[128,4,2048]{2,1,0:T(4,128)(2,1)}, u32[]{:S(2)}) copy-start(bf16[128,4,2048]{2,1,0:T(4,128)(2,1)} %get-tuple-element.6) | copy-start | bytes 6291460
where the time goes:
time: 71.2 us; the launch traced here: 71 us
  Pallas kernels  62.5 us (88%)
  local copies, waits for them, and re-layouts  7.87 us (11%)
    pallas_call x1, Pallas kernels, layer(): pl.pallas_call(kernel, out_shape=(jax.ShapeDtypeStruct((128, 4, 2048), BF...  62.5 us
    unnamed x5, local copies, waits for them, and re-layouts  5.23 us
    pallas_call x1, local copies, waits for them, and re-layouts, layer(): pl.pallas_call(kernel, out_shape=(jax.ShapeDtypeStruct((128, 4, 2048), BF...  2.64 us

commit v1 on v0

--- a/solution.py
+++ b/solution.py
@@ -32,8 +32,8 @@
 def kernel(
     x_hbm, gain, pw, gw, qw, kw, vw, aw, mix, qg, kg, sink, outp, outa,
     out, lse,
-    xb, wb, kst, vst, tmp, qs, kvs, poolbuf, gate, agate, bias, band, ysend, yr, wg, acc, att, lseb,
-    xsem, wsem, asend, arecv, hsend, hrecv, gsend, grecv, dsend, drecv,
+    xa, xc, xo, wb, kvt, pa, pc, tmp, inv, rsend, rbuf, qs, kvs, poolbuf, gate, agate, bias, band, ysend, yr, wg, acc, att,
+    xsem, wsem, rs_send, rs_recv, asend, arecv, hsend, hrecv, gsend, grecv, dsend, drecv,
 ):
     if COMM:
         sp = lax.axis_index("sp")
@@ -55,8 +55,11 @@
 
     def xcopy(k):
         return pltpu.make_async_copy(
-            x_hbm.at[pl.ds(order(k) * 128, 128)], xb.at[k % 2], xsem.at[k % 2]
-        )
+            x_hbm.at[pl.ds(order(k) * 128, 128)], (xa, xc)[k % 2], xsem.at[k % 2]
+        )
+
+    xown = pltpu.make_async_copy(x_hbm.at[pl.ds(tp * 128, 128)], xo, xsem.at[2])
+    xown.start()
 
     wcopies = [
         pltpu.make_async_copy(outp, wg.at[0, sp], wsem.at[0]),
@@ -64,8 +67,8 @@
         pltpu.make_async_copy(pw, wb.at[:, pl.ds(0, 128)], wsem.at[2]),
         pltpu.make_async_copy(gw, wb.at[:, pl.ds(128, 128)], wsem.at[3]),
         pltpu.make_async_copy(qw, wb.at[:, pl.ds(256, 128)], wsem.at[4]),
-        pltpu.make_async_copy(kw, kst, wsem.at[5]),
-        pltpu.make_async_copy(vw, vst, wsem.at[6]),
+        pltpu.make_async_copy(kw, kvt.at[pl.ds(0, 64)], wsem.at[5]),
+        pltpu.make_async_copy(vw, kvt.at[pl.ds(64, 64)], wsem.at[6]),
         pltpu.make_async_copy(aw, wb.at[:, pl.ds(512, 128)], wsem.at[7]),
     ]
     for cp in wcopies:
@@ -101,7 +104,9 @@
 
         greet(((sp + 1) % NSP, tp))
         greet(((sp + NSP - 1) % NSP, tp))
-        pl.semaphore_wait(barrier, 13)
+
+    sp0 = 1 - (sp + 15) // 16
+    sp15 = (sp + 1) // 16
 
     def slice_at(da, db):
         return ((a + da) % 4) * sa + ((b_ + db) % 4) * sb
@@ -193,17 +198,43 @@
     def event5():
         far(2)
 
+    lane = lax.broadcasted_iota(jnp.int32, (1, 128), 1)
+    low = lane < 64
+    ones = jnp.ones((128, 128), BF)
+    row128 = lax.broadcasted_iota(jnp.int32, (128, 128), 0)
+    col128 = lax.broadcasted_iota(jnp.int32, (128, 128), 1)
+    head_ones = ((row128 // 64) == (col128 // 64)).astype(F32).astype(BF)
+
+    xown.wait()
+    x = xo[...].reshape(512, 2048)
+    sq = jnp.zeros((512, 128), F32)
+    for l in range(16):
+        t = x[:, 128 * l : 128 * l + 128].astype(F32)
+        sq = sq + t * t
+    r = lax.rsqrt(split_dot(sq, ones) * (1.0 / 2048) + EPS)
+    packed = [
+        jnp.sum(jnp.where(row128 == col128, r[128 * g : 128 * g + 128], 0.0), axis=0, keepdims=True)
+        for g in range(4)
+    ]
+    packed = jnp.concatenate(packed + [jnp.zeros((4, 128), F32)], axis=0)
+    rsend[...] = packed
+    rbuf[tp] = packed
+
+    def rcopy(j, at):
+        return remote(rsend, rbuf.at[at], rs_send.at[j], rs_recv.at[at], (sp, j))
+
+    if COMM:
+        pl.semaphore_wait(barrier, 13)
+
+    if COMM:
+        for j in range(8):
+            @pl.when(tp != j)
+            def _():
+                rcopy(j, tp).start()
+
     wcopies[0].wait()
     wcopies[1].wait()
     event0()
-
-    lane = lax.broadcasted_iota(jnp.int32, (1, 128), 1)
-    low = lane < 64
-    ones = jnp.ones((128, 128), BF)
-    head_ones = (
-        (lax.broadcasted_iota(jnp.int32, (128, 128), 0) // 64)
-        == (lax.broadcasted_iota(jnp.int32, (128, 128), 1) // 64)
-    ).astype(F32).astype(BF)
 
     tpf = tp.astype(F32)
     s0 = sink[0]
@@ -231,6 +262,16 @@
         ((delta + 1024) % 4 == 0) & (delta >= -4 * hw) & (delta <= 4 * hw - 4)
     ).astype(F32).astype(BF)
 
+    for e in range(3):
+        pos = lax.broadcasted_iota(jnp.int32, (512, 128), 0) // 4
+        lo = pos - hw
+        hi = pos + hw - 1
+        if e == 1:
+            lo = jnp.maximum(lo, 0)
+        if e == 2:
+            hi = jnp.minimum(hi, 127)
+        inv[e] = 1.0 / (hi - lo + 1).astype(F32)
+
     for cp in wcopies[2:]:
         cp.wait()
 
@@ -240,11 +281,11 @@
         for t in (0, 1, 2, 4):
             cols = slice(128 * t, 128 * t + 128)
             wb[rows, cols] = (wb[rows, cols].astype(F32) * g).astype(BF)
-        kv = jnp.concatenate([kst[rows, :].astype(F32), vst[rows, :].astype(F32)], axis=1)
+        kv = jnp.transpose(kvt[:, rows].astype(F32))
         wb[rows, 384:512] = (kv * g).astype(BF)
         return carry
 
-    lax.fori_loop(0, 16, prep, 0)
+    lax.fori_loop(0, 16, prep, 0, unroll=2)
 
     qgain = jnp.concatenate([qg[...], qg[...]], axis=1) * (0.125 * LOG2E)
     kgain = jnp.concatenate([kg[...], kg[...]], axis=1)
@@ -264,15 +305,29 @@
             halo(3, poolbuf.at[pl.ds(64 + 4096 - 32, 32)], poolbuf.at[pl.ds(32, 32)], (sp + 1, tp)),
         )
 
-    def project(k, blk):
-        xcopy(k).wait()
-        x = xb[k % 2].reshape(512, 2048)
-        sq = jnp.zeros((512, 128), F32)
-        for l in range(16):
-            t = x[:, 128 * l : 128 * l + 128].astype(F32)
-            sq = sq + t * t
-        r = lax.rsqrt(split_dot(sq, ones) * (1.0 / 2048) + EPS)
-        p = jnp.dot(x, wb[...], preferred_element_type=F32)
+    def multiply(k):
+        p = (pa, pc)[k % 2]
+        x = (xa, xc)[k % 2][...].reshape(512, 2048)
+        p[...] = jnp.dot(x, wb[...], preferred_element_type=F32)
+
+    def ready(k):
+        if COMM:
+            blk = order(k)
+
+            @pl.when(blk != tp)
+            def _():
+                rcopy(blk, blk).wait_recv()
+
+    def finish(k):
+        blk = order(k)
+        p = (pa, pc)[k % 2]
+        r = jnp.concatenate(
+            [
+                jnp.transpose(jnp.broadcast_to(rbuf[blk, g : g + 1, :], (128, 128)))
+                for g in range(4)
+            ],
+            axis=0,
+        )
         rows = pl.ds(pl.multiple_of(blk * 512, 512), 512)
         prows = pl.ds(pl.multiple_of(blk * 512 + 64, 64), 512)
         poolbuf[prows, :] = (p[:, 0:128] * r).astype(BF)
@@ -292,11 +347,10 @@
                 1, pl.ds(s, 128, stride=4), :
             ].astype(BF)
 
-        @pl.when(k + 2 < 8)
-        def _():
-            xcopy(k + 2).start()
-
-        if COMM:
+    def edges(k):
+        if COMM:
+            blk = order(k)
+
             @pl.when((blk == 0) & (sp > 0))
             def _():
                 for cp in halo_left():
@@ -307,29 +361,25 @@
                 for cp in halo_right():
                     cp.start()
 
-    def emit(part, blk, value):
-        @pl.when(blk == tp)
-        def _():
-            yr[part, blk] = value
-
-        @pl.when(blk != tp)
-        def _():
-            ysend[part, blk] = value
-            if COMM:
+    def emit(part, blk):
+        if COMM:
+            @pl.when(blk != tp)
+            def _():
                 remote(
                     ysend.at[part, blk], yr.at[part, tp], asend.at[part, blk], arecv.at[part, tp], (sp, blk)
                 ).start()
 
+    def pool_wait(blk):
+        if COMM:
+            @pl.when((blk == 0) & (sp > 0))
+            def _():
+                halo_right()[1].wait_recv()
+
+            @pl.when((blk == 7) & (sp < NSP - 1))
+            def _():
+                halo_left()[1].wait_recv()
+
     def pool(blk):
-        if COMM:
-            @pl.when((blk == 0) & (sp > 0))
-            def _():
-                halo_right()[1].wait_recv()
-
-            @pl.when((blk == 7) & (sp < NSP - 1))
-            def _():
-                halo_left()[1].wait_recv()
-
         start = pl.multiple_of(blk * 512, 512)
         sums = jnp.concatenate(
             [
@@ -338,38 +388,47 @@
             ],
             axis=0,
         )
-        pos = sp * 1024 + blk * 128 + lax.broadcasted_iota(jnp.int32, (512, 128), 0) // 4
-        lo = jnp.maximum(pos - hw, 0)
-        hi = jnp.minimum(pos + hw - 1, SEQ_LEN - 1)
-        count = (hi - lo + 1).astype(F32)
+        scale = inv[sp0 * (1 - (blk + 7) // 8) + 2 * sp15 * ((blk + 1) // 8)]
         own = poolbuf[pl.ds(start + 64, 512), :].astype(F32)
-        pooled = (sums / count - own).astype(BF)
+        pooled = (sums * scale - own).astype(BF)
         mixed = jnp.dot(pooled, mix[0], preferred_element_type=F32)
         g = gate[pl.ds(start, 512), :].astype(F32)
-        emit(0, blk, (mixed * silu(g)).astype(BF))
-
-    def proj_step(k, carry):
-        project(k, order(k))
-
-        @pl.when(k >= 3)
-        def _():
-            pool(order(k - 2))
-
-        if COMM:
-            for at, event in ((2, event1), (4, event2), (6, event3)):
-                pl.when(k == at)(event)
+        ysend[0, blk] = (mixed * silu(g)).astype(BF)
+
+    def step(k, top, pooling):
+        if top:
+            xcopy(k).wait()
+        if k > 0:
+            ready(k - 1)
+        if pooling:
+            pool_wait(order(k - 3))
+        if top:
+            multiply(k)
+        if k > 0:
+            finish(k - 1)
+        if pooling:
+            pool(order(k - 3))
+        if top and k + 2 < 8:
+            xcopy(k + 2).start()
+        if k > 0:
+            edges(k - 1)
+        if pooling:
+            emit(0, order(k - 3))
+
+    for k in range(8):
+        step(k, True, k >= 4)
+        if COMM and k in (2, 4, 6):
+            {2: event1, 4: event2, 6: event3}[k]()
+    step(8, False, True)
+
+    def pool_rest(k, carry):
+        blk = order(k % 8)
+        pool_wait(blk)
+        pool(blk)
+        emit(0, blk)
         return carry
 
-    lax.fori_loop(0, 8, proj_step, 0)
-
-    def pool_rest(k, carry):
-        pool(order(k % 8))
-        return carry
-
     lax.fori_loop(6, 9, pool_rest, 0)
-
-    sp0 = 1 - (sp + 15) // 16
-    sp15 = (sp + 1) // 16
 
     def attend(blk):
         if COMM:
@@ -396,18 +455,16 @@
             )
             rhs = jnp.concatenate([kv, jnp.ones((384, 128), BF)], axis=1)
             o = jnp.dot(w, rhs, preferred_element_type=F32)
-            t0 = o[0:128, 128:256] + jnp.exp(jnp.full((128, 128), s0 - m0, F32))
-            t1 = o[128:256, 128:256] + jnp.exp(jnp.full((128, 128), s1 - m1, F32))
-            both = jnp.where(
-                low, pltpu.roll(o[0:128, 0:128], 64, 1) / t0, o[128:256, 0:128] / t1
-            )
-            att[pl.ds(s, 128, stride=4), :] = both
-            lseb[pl.ds(s, 128, stride=4), :] = jnp.where(
-                lane == 0, m0 + jnp.log(t0), m1 + jnp.log(t1)
-            )
+            t0 = o[0:128, 128:256] + jnp.exp(jnp.full((1, 128), s0 - m0, F32))
+            t1 = o[128:256, 128:256] + jnp.exp(jnp.full((1, 128), s1 - m1, F32))
+            over = jnp.where(low, pltpu.roll(o[0:128, 0:128], 64, 1), o[128:256, 0:128])
+            att[pl.ds(s, 128, stride=4), :] = over / jnp.where(low, t0, t1)
+            totals = jnp.log(jnp.transpose(jnp.where(lane == 0, t0, t1))[0:2, :])
+            top = jnp.where(lax.broadcasted_iota(jnp.int32, (2, 128), 0) == 0, m0, m1)
+            lse[s, :, pl.ds(pl.multiple_of(blk * 128, 128), 128)] = top + totals
         g = agate[pl.ds(pl.multiple_of(blk * 512, 512), 512), :].astype(F32)
-        emit(1, blk, (att[...] * silu(g)).astype(BF))
-        lse[pl.ds(pl.multiple_of(blk * 128, 128), 128)] = lseb[:, 0:2].reshape(128, 4, 2)
+        ysend[1, blk] = (att[...] * silu(g)).astype(BF)
+        emit(1, blk)
 
     def att_step(k, carry):
         j = k // 2
@@ -444,29 +501,32 @@
                         ref, ref, dsend.at[da * 4 + db], drecv.at[da * 4 + db], (sp, tp + 1 - 2 * c)
                     ).wait_recv()
 
+    for part in range(2):
+        yr[part, tp] = ysend[part, tp]
+
     arrive(0)
 
     def out_pool_step(n, carry):
-        cols = pl.ds(pl.multiple_of(n * 256, 256), 256)
+        cols = pl.ds(pl.multiple_of(n * 512, 512), 512)
         acts = jnp.concatenate([yr[0, j] for j in range(8)], axis=1)
         acc[:, cols] = jnp.dot(
-            acts, wg[0, :, :, cols].reshape(1024, 256), preferred_element_type=F32
+            acts, wg[0, :, :, cols].reshape(1024, 512), preferred_element_type=F32
         )
         return carry
 
-    lax.fori_loop(0, 8, out_pool_step, 0)
+    lax.fori_loop(0, 4, out_pool_step, 0)
     arrive(1)
 
     def out_attn_step(n, carry):
-        cols = pl.ds(pl.multiple_of(n * 256, 256), 256)
+        cols = pl.ds(pl.multiple_of(n * 512, 512), 512)
         acts = jnp.concatenate([yr[1, j] for j in range(8)], axis=1)
         total = acc[:, cols] + jnp.dot(
-            acts, wg[1, :, :, cols].reshape(1024, 256), preferred_element_type=F32
-        )
-        out[:, :, cols] = total.astype(BF).reshape(128, 4, 256)
+            acts, wg[1, :, :, cols].reshape(1024, 512), preferred_element_type=F32
+        )
+        out[:, :, cols] = total.astype(BF).reshape(128, 4, 512)
         return carry
 
-    lax.fori_loop(0, 8, out_attn_step, 0)
+    lax.fori_loop(0, 4, out_attn_step, 0)
 
     if COMM:
         for part in range(2):
@@ -474,6 +534,10 @@
                 @pl.when(tp != j)
                 def _():
                     exchange(part, j).wait_send()
+        for j in range(8):
+            @pl.when(tp != j)
+            def _():
+                rcopy(j, tp).wait_send()
         for item in sends:
             gcopy(*item).wait_send()
         for da in range(4):
@@ -500,20 +564,26 @@
     vmem = pl.BlockSpec(memory_space=pltpu.VMEM)
     smem = pl.BlockSpec(memory_space=pltpu.SMEM)
     dma = pltpu.SemaphoreType.DMA
-    return pl.pallas_call(
+    mixed, log_sums = pl.pallas_call(
         kernel,
         out_shape=(
             jax.ShapeDtypeStruct((128, 4, 2048), BF),
-            jax.ShapeDtypeStruct((1024, 4, 2), F32),
+            jax.ShapeDtypeStruct((4, 2, 1024), F32),
         ),
         in_specs=[hbm, vmem, hbm, hbm, hbm, hbm, hbm, hbm, vmem, vmem, vmem, smem, hbm, hbm],
         out_specs=(vmem, vmem),
         scratch_shapes=[
-            pltpu.VMEM((2, 128, 4, 2048), BF),
+            pltpu.VMEM((128, 4, 2048), BF),
+            pltpu.VMEM((128, 4, 2048), BF),
+            pltpu.VMEM((128, 4, 2048), BF),
             pltpu.VMEM((2048, 640), BF),
-            pltpu.VMEM((2048, 64), BF),
-            pltpu.VMEM((2048, 64), BF),
+            pltpu.VMEM((128, 2048), BF),
+            pltpu.VMEM((512, 640), F32),
+            pltpu.VMEM((512, 640), F32),
             pltpu.VMEM((2, 512, 128), F32),
+            pltpu.VMEM((3, 512, 128), F32),
+            pltpu.VMEM((8, 128), F32),
+            pltpu.VMEM((8, 8, 128), F32),
             pltpu.VMEM((8, 4, 256, 128), BF),
             pltpu.VMEM((4, 1280, 128), BF),
             pltpu.VMEM((4096 + 128, 128), BF),
@@ -526,8 +596,7 @@
             pltpu.VMEM((2, 16, 64, 2048), BF),
             pltpu.VMEM((512, 2048), F32),
             pltpu.VMEM((512, 128), F32),
-            pltpu.VMEM((512, 128), F32),
-            dma((2,)), dma((8,)),
+            dma((3,)), dma((8,)), dma((8,)), dma((8,)),
             dma((2, 8)), dma((2, 8)),
             dma((4,)), dma((4,)),
             dma((24,)), dma((16, 2)),
@@ -539,10 +608,11 @@
         ),
         name="mixer_layer",
     )(
-        inputs, norm_gain.reshape(16, 128), pool_proj, pool_gate_proj, query_proj, key_proj,
-        value_proj, attn_gate_proj, pool_mix, query_gain.reshape(1, 64), key_gain.reshape(1, 64),
+        inputs, norm_gain.reshape(16, 128), pool_proj, pool_gate_proj, query_proj, key_proj.T,
+        value_proj.T, attn_gate_proj, pool_mix, query_gain.reshape(1, 64), key_gain.reshape(1, 64),
         sink_logit, out_pool, out_attn,
     )
+    return mixed, jnp.transpose(log_sums, (2, 0, 1))
 
 
 def solution(mesh):

time: 71.2 us -> 64.5 us (0.906); the launches traced: 71 us -> 63.2 us
  Pallas kernels: 62.5 us -> 58 us
  local copies, waits for them, and re-layouts: 7.87 us -> 4.54 us
    pallas_call x1, Pallas kernels: 62.5 us -> 58 us  [layer(): pl.pallas_call(kernel, out_shape=(jax.ShapeDtypeStruct((128, 4, 2048), BF...]
    pallas_call x1 -> x0, local copies, waits for them, and re-layouts: 2.64 us -> none  [layer(): pl.pallas_call(kernel, out_shape=(jax.ShapeDtypeStruct((128, 4, 2048), BF...]
    unnamed x5 -> x4, local copies, waits for them, and re-layouts: 5.23 us -> 4.54 us
where the time goes in v1:
time: 64.5 us; the launch traced here: 63.2 us
  Pallas kernels  58 us (90%)
  local copies, waits for them, and re-layouts  4.54 us (7%)
  between operations  0.65 us (1%)
    pallas_call x1, Pallas kernels, layer(): pl.pallas_call(kernel, out_shape=(jax.ShapeDtypeStruct((128, 4, 2048), BF...  58 us
    unnamed x4, local copies, waits for them, and re-layouts  4.54 us

profile of v1, /device:TPU:33, one launch (start us, length us, event | category | flops | bytes accessed | tf_op | source)
XLA Modules:
  0.0 63.2 jit_solution(16016522808762437357)
XLA Ops:
  0.6 58.0 %mixer_layer.1 = (bf16[128,4,2048]{2,1,0:T(4,128)(2,1)}, f32[4,2,1024]{2,1,0:T(2,128)}) custom-call(bf16[1024,4,2048]{2,1,0:T(4,128)(2,1)} %x_hbm.1, f32[16,128]{1,0:T(8,128)} %bitcast.9, bf16[2048,128]{1,0:T(8,128)(2,1)} %pw.1, bf16[2048,128]{1,0:T(8,128)(2,1)} %gw.1, bf16[2048,128]{1,0:T(8,128)(2,1)} %qw.1, bf16[64,2048]{1,0:T(8,128)(2,1)} %bitcast.6, ...), custom_call_target="tpu_custom_call" | custom-call | tf_op jit(solution)/shard_map/mixer_layer/pallas_call | solution.py:567
  58.7 0.0 copy-start
  58.7 3.9 %copy.18 = bf16[128,4,2048]{2,1,0:T(4,128)(2,1)} copy(bf16[128,4,2048]{2,1,0:T(4,128)(2,1)} %get-tuple-element.8) | data formatting | bytes 4194304
  62.6 0.0 copy-done
  62.6 0.6 copy.19
Async XLA Ops:
  58.7 3.9 %copy-start = (f32[4,2,1024]{2,1,0:T(2,128)S(1)}, f32[4,2,1024]{2,1,0:T(2,128)}, u32[]{:S(2)}) copy-start(f32[4,2,1024]{2,1,0:T(2,128)} %get-tuple-element.5) | copy-start | bytes 98308

commit v2 on v1

--- a/solution.py
+++ b/solution.py
@@ -17,6 +17,8 @@
 SEQ_LEN = 16384
 NSP = 16
 COMM = True
+NEAR = (0, 2)
+FAR = (1, 3)
 
 
 def split_dot(values, ones):
@@ -32,8 +34,8 @@
 def kernel(
     x_hbm, gain, pw, gw, qw, kw, vw, aw, mix, qg, kg, sink, outp, outa,
     out, lse,
-    xa, xc, xo, wb, kvt, pa, pc, tmp, inv, rsend, rbuf, qs, kvs, poolbuf, gate, agate, bias, band, ysend, yr, wg, acc, att,
-    xsem, wsem, rs_send, rs_recv, asend, arecv, hsend, hrecv, gsend, grecv, dsend, drecv,
+    xa, xc, xo, xe, edge, wb, kvt, pa, pc, tmp, inv, rsend, rbuf, qs, kvs, poolbuf, gate, agate, bias, band, ysend, yr, wg, acc, att, relay,
+    xsem, wsem, rs_send, rs_recv, lsend, lrecv, asend, arecv, hsend, hrecv, gsend, grecv, dsend, drecv,
 ):
     if COMM:
         sp = lax.axis_index("sp")
@@ -51,7 +53,7 @@
     sb = 4 - 3 * c
 
     def order(k):
-        return (2 * chip + 1 - c + k - 2 * c * k + 16) % 8
+        return (2 * chip + 1 - c + (k + 2) - 2 * c * (k + 2) + 16) % 8
 
     def xcopy(k):
         return pltpu.make_async_copy(
@@ -60,6 +62,12 @@
 
     xown = pltpu.make_async_copy(x_hbm.at[pl.ds(tp * 128, 128)], xo, xsem.at[2])
     xown.start()
+    xedge = (
+        pltpu.make_async_copy(x_hbm.at[pl.ds(0, 8)], xe.at[pl.ds(0, 8)], xsem.at[3]),
+        pltpu.make_async_copy(x_hbm.at[pl.ds(1016, 8)], xe.at[pl.ds(8, 8)], xsem.at[4]),
+    )
+    for cp in xedge:
+        cp.start()
 
     wcopies = [
         pltpu.make_async_copy(outp, wg.at[0, sp], wsem.at[0]),
@@ -192,10 +200,12 @@
 
     def event4():
         through(2)
+
+    def event5():
         far(3)
         far(1)
 
-    def event5():
+    def event6():
         far(2)
 
     lane = lax.broadcasted_iota(jnp.int32, (1, 128), 1)
@@ -204,37 +214,6 @@
     row128 = lax.broadcasted_iota(jnp.int32, (128, 128), 0)
     col128 = lax.broadcasted_iota(jnp.int32, (128, 128), 1)
     head_ones = ((row128 // 64) == (col128 // 64)).astype(F32).astype(BF)
-
-    xown.wait()
-    x = xo[...].reshape(512, 2048)
-    sq = jnp.zeros((512, 128), F32)
-    for l in range(16):
-        t = x[:, 128 * l : 128 * l + 128].astype(F32)
-        sq = sq + t * t
-    r = lax.rsqrt(split_dot(sq, ones) * (1.0 / 2048) + EPS)
-    packed = [
-        jnp.sum(jnp.where(row128 == col128, r[128 * g : 128 * g + 128], 0.0), axis=0, keepdims=True)
-        for g in range(4)
-    ]
-    packed = jnp.concatenate(packed + [jnp.zeros((4, 128), F32)], axis=0)
-    rsend[...] = packed
-    rbuf[tp] = packed
-
-    def rcopy(j, at):
-        return remote(rsend, rbuf.at[at], rs_send.at[j], rs_recv.at[at], (sp, j))
-
-    if COMM:
-        pl.semaphore_wait(barrier, 13)
-
-    if COMM:
-        for j in range(8):
-            @pl.when(tp != j)
-            def _():
-                rcopy(j, tp).start()
-
-    wcopies[0].wait()
-    wcopies[1].wait()
-    event0()
 
     tpf = tp.astype(F32)
     s0 = sink[0]
@@ -272,6 +251,40 @@
             hi = jnp.minimum(hi, 127)
         inv[e] = 1.0 / (hi - lo + 1).astype(F32)
 
+    if COMM:
+        pl.semaphore_wait(barrier, 13)
+
+    wcopies[0].wait()
+    wcopies[1].wait()
+    event0()
+
+    def row_scale(x):
+        sq = jnp.zeros((x.shape[0], 128), F32)
+        for l in range(16):
+            t = x[:, 128 * l : 128 * l + 128].astype(F32)
+            sq = sq + t * t
+        return lax.rsqrt(split_dot(sq, ones) * (1.0 / 2048) + EPS)
+
+    xown.wait()
+    r = row_scale(xo[...].reshape(512, 2048))
+    packed = [
+        jnp.sum(jnp.where(row128 == col128, r[128 * g : 128 * g + 128], 0.0), axis=0, keepdims=True)
+        for g in range(4)
+    ]
+    packed = jnp.concatenate(packed + [jnp.zeros((4, 128), F32)], axis=0)
+    rsend[...] = packed
+    rbuf[tp] = packed
+
+    def rcopy(j, at):
+        return remote(rsend, rbuf.at[at], rs_send.at[j], rs_recv.at[at], (sp, j))
+
+    if COMM:
+        for j in range(8):
+            @pl.when(tp != j)
+            def _():
+                rcopy(j, tp).start()
+
+
     for cp in wcopies[2:]:
         cp.wait()
 
@@ -296,19 +309,34 @@
     def halo_left():
         return (
             halo(0, kvs.at[:, pl.ds(128, 128), :], kvs.at[:, pl.ds(9 * 128, 128), :], (sp - 1, tp)),
-            halo(1, poolbuf.at[pl.ds(64, 32)], poolbuf.at[pl.ds(64 + 4096, 32)], (sp - 1, tp)),
+            halo(1, edge.at[pl.ds(0, 32)], poolbuf.at[pl.ds(64 + 4096, 32)], (sp - 1, tp)),
         )
 
     def halo_right():
         return (
             halo(2, kvs.at[:, pl.ds(8 * 128, 128), :], kvs.at[:, pl.ds(0, 128), :], (sp + 1, tp)),
-            halo(3, poolbuf.at[pl.ds(64 + 4096 - 32, 32)], poolbuf.at[pl.ds(32, 32)], (sp + 1, tp)),
-        )
-
-    def multiply(k):
+            halo(3, edge.at[pl.ds(32, 32)], poolbuf.at[pl.ds(32, 32)], (sp + 1, tp)),
+        )
+
+    for cp in xedge:
+        cp.wait()
+    x = xe[...].reshape(64, 2048)
+    edge[...] = (
+        jnp.dot(x, wb[:, 0:128], preferred_element_type=F32) * row_scale(x)
+    ).astype(BF)
+    if COMM:
+        @pl.when(sp > 0)
+        def _():
+            halo_left()[1].start()
+
+        @pl.when(sp < NSP - 1)
+        def _():
+            halo_right()[1].start()
+
+    def multiply(k, lo, hi):
         p = (pa, pc)[k % 2]
         x = (xa, xc)[k % 2][...].reshape(512, 2048)
-        p[...] = jnp.dot(x, wb[...], preferred_element_type=F32)
+        p[:, lo:hi] = jnp.dot(x, wb[:, lo:hi], preferred_element_type=F32)
 
     def ready(k):
         if COMM:
@@ -318,21 +346,28 @@
             def _():
                 rcopy(blk, blk).wait_recv()
 
-    def finish(k):
+    def scales(k):
         blk = order(k)
-        p = (pa, pc)[k % 2]
-        r = jnp.concatenate(
+        return jnp.concatenate(
             [
                 jnp.transpose(jnp.broadcast_to(rbuf[blk, g : g + 1, :], (128, 128)))
                 for g in range(4)
             ],
             axis=0,
         )
+
+    def finish_gates(k, r):
+        blk = order(k)
+        p = (pa, pc)[k % 2]
         rows = pl.ds(pl.multiple_of(blk * 512, 512), 512)
         prows = pl.ds(pl.multiple_of(blk * 512 + 64, 64), 512)
         poolbuf[prows, :] = (p[:, 0:128] * r).astype(BF)
         gate[rows, :] = (p[:, 128:256] * r).astype(BF)
         agate[rows, :] = (p[:, 512:640] * r).astype(BF)
+
+    def finish_heads(k, r):
+        blk = order(k)
+        p = (pa, pc)[k % 2]
         q = (p[:, 256:384] * r).astype(BF).astype(F32)
         rq = lax.rsqrt(split_dot(q * q, head_ones) * (1.0 / 64) + EPS)
         tmp[0] = q * rq * qgain
@@ -353,21 +388,52 @@
 
             @pl.when((blk == 0) & (sp > 0))
             def _():
-                for cp in halo_left():
-                    cp.start()
+                halo_left()[0].start()
 
             @pl.when((blk == 7) & (sp < NSP - 1))
             def _():
-                for cp in halo_right():
-                    cp.start()
+                halo_right()[0].start()
+
+    def ahead(part):
+        return (chip + 1 + 2 * ((c + part) % 2)) % 4
+
+    def behind(part):
+        return ((chip + 3 + 2 * ((c + part) % 2)) % 4) * 2 + c
+
+    def direct(part, blk):
+        return remote(
+            ysend.at[part, blk], yr.at[part, tp], asend.at[part, blk], arecv.at[part, tp], (sp, blk)
+        )
+
+    def first_hop(part, blk):
+        return remote(
+            ysend.at[part, blk], relay.at[part, blk % 2], asend.at[part, blk], lrecv.at[part, blk % 2],
+            (sp, ahead(part) * 2 + c),
+        )
+
+    def second_hop(part, e):
+        return remote(
+            relay.at[part, e], yr.at[part, behind(part)], lsend.at[part, e], arecv.at[part, behind(part)],
+            (sp, ahead(part) * 2 + e),
+        )
+
+    def away(blk):
+        return (blk // 2 - chip + 4) % 4
 
     def emit(part, blk):
         if COMM:
-            @pl.when(blk != tp)
-            def _():
-                remote(
-                    ysend.at[part, blk], yr.at[part, tp], asend.at[part, blk], arecv.at[part, tp], (sp, blk)
-                ).start()
+            @pl.when((blk != tp) & (away(blk) != 2))
+            def _():
+                direct(part, blk).start()
+
+            @pl.when(away(blk) == 2)
+            def _():
+                first_hop(part, blk).start()
+
+    def pass_on(part, e):
+        if COMM:
+            first_hop(part, e).wait_recv()
+            second_hop(part, e).start()
 
     def pool_wait(blk):
         if COMM:
@@ -401,24 +467,39 @@
         if k > 0:
             ready(k - 1)
         if pooling:
-            pool_wait(order(k - 3))
+            pool_wait(order(k - 2))
         if top:
-            multiply(k)
+            multiply(k, 0, 256)
         if k > 0:
-            finish(k - 1)
+            r = scales(k - 1)
+            finish_gates(k - 1, r)
+        if top:
+            multiply(k, 256, 512)
+        if k > 0:
+            finish_heads(k - 1, r)
+        if top:
+            multiply(k, 512, 640)
         if pooling:
-            pool(order(k - 3))
+            pool(order(k - 2))
         if top and k + 2 < 8:
             xcopy(k + 2).start()
         if k > 0:
             edges(k - 1)
         if pooling:
-            emit(0, order(k - 3))
+            emit(0, order(k - 2))
 
     for k in range(8):
-        step(k, True, k >= 4)
-        if COMM and k in (2, 4, 6):
-            {2: event1, 4: event2, 6: event3}[k]()
+        step(k, True, k >= 3)
+        if k == 1:
+            event1()
+        if k == 3:
+            event2()
+        if k == 6:
+            event3()
+        if k == 5:
+            pass_on(0, c)
+        if k == 6:
+            pass_on(0, 1 - c)
     step(8, False, True)
 
     def pool_rest(k, carry):
@@ -428,7 +509,8 @@
         emit(0, blk)
         return carry
 
-    lax.fori_loop(6, 9, pool_rest, 0)
+    lax.fori_loop(7, 9, pool_rest, 0)
+    event4()
 
     def attend(blk):
         if COMM:
@@ -472,25 +554,24 @@
         d = (d + c * (4 - 2 * d)) % 4
         attend(((chip + d) % 4) * 2 + (c + 1 + k) % 2)
         if COMM:
-            for at, event in ((1, event4), (5, event5)):
+            for at, event in (
+                (3, event5),
+                (4, functools.partial(pass_on, 1, (c + 1) % 2)),
+                (5, event6),
+                (6, functools.partial(pass_on, 1, c)),
+            ):
                 pl.when(k == at)(event)
         return carry
 
     lax.fori_loop(0, 8, att_step, 0)
 
-    def exchange(part, j):
-        return remote(
-            ysend.at[part, j], yr.at[part, tp], asend.at[part, j], arecv.at[part, j], (sp, j)
-        )
-
-    def arrive(part):
-        if COMM:
-            for j in range(8):
-                @pl.when(tp != j)
-                def _():
-                    remote(
-                        ysend.at[part, j], yr.at[part, j], asend.at[part, j], arecv.at[part, j], (sp, j)
-                    ).wait_recv()
+    def arrive(part, j):
+        if COMM:
+            @pl.when(tp != j)
+            def _():
+                remote(
+                    ysend.at[part, j], yr.at[part, j], asend.at[part, j], arecv.at[part, j], (sp, j)
+                ).wait_recv()
 
     if COMM:
         for da in range(4):
@@ -504,7 +585,8 @@
     for part in range(2):
         yr[part, tp] = ysend[part, tp]
 
-    arrive(0)
+    for j in range(8):
+        arrive(0, j)
 
     def out_pool_step(n, carry):
         cols = pl.ds(pl.multiple_of(n * 512, 512), 512)
@@ -515,17 +597,30 @@
         return carry
 
     lax.fori_loop(0, 4, out_pool_step, 0)
-    arrive(1)
+
+    def attn_part(cols, d):
+        src = [(chip + e) % 4 for e in d]
+        acts = jnp.concatenate([yr[1, 2 * e + h] for e in src for h in range(2)], axis=1)
+        rows = jnp.concatenate([wg[1, pl.ds(4 * e, 4), :, cols].reshape(256, 512) for e in src], axis=0)
+        return acc[:, cols] + jnp.dot(acts, rows, preferred_element_type=F32)
+
+    def out_near_step(n, carry):
+        cols = pl.ds(pl.multiple_of(n * 512, 512), 512)
+        acc[:, cols] = attn_part(cols, NEAR)
+        return carry
 
     def out_attn_step(n, carry):
         cols = pl.ds(pl.multiple_of(n * 512, 512), 512)
-        acts = jnp.concatenate([yr[1, j] for j in range(8)], axis=1)
-        total = acc[:, cols] + jnp.dot(
-            acts, wg[1, :, :, cols].reshape(1024, 512), preferred_element_type=F32
-        )
-        out[:, :, cols] = total.astype(BF).reshape(128, 4, 512)
+        out[:, :, cols] = attn_part(cols, FAR).astype(BF).reshape(128, 4, 512)
         return carry
 
+    for d in NEAR:
+        for h in range(2):
+            arrive(1, 2 * ((chip + d) % 4) + h)
+    lax.fori_loop(0, 4, out_near_step, 0)
+    for d in FAR:
+        for h in range(2):
+            arrive(1, 2 * ((chip + d) % 4) + h)
     lax.fori_loop(0, 4, out_attn_step, 0)
 
     if COMM:
@@ -533,11 +628,14 @@
             for j in range(8):
                 @pl.when(tp != j)
                 def _():
-                    exchange(part, j).wait_send()
+                    direct(part, j).wait_send()
         for j in range(8):
             @pl.when(tp != j)
             def _():
                 rcopy(j, tp).wait_send()
+        for part in range(2):
+            for e in range(2):
+                second_hop(part, e).wait_send()
         for item in sends:
             gcopy(*item).wait_send()
         for da in range(4):
@@ -567,8 +665,8 @@
     mixed, log_sums = pl.pallas_call(
         kernel,
         out_shape=(
-            jax.ShapeDtypeStruct((128, 4, 2048), BF),
-            jax.ShapeDtypeStruct((4, 2, 1024), F32),
+            pltpu.VMEM((128, 4, 2048), BF),
+            pltpu.VMEM((4, 2, 1024), F32),
         ),
         in_specs=[hbm, vmem, hbm, hbm, hbm, hbm, hbm, hbm, vmem, vmem, vmem, smem, hbm, hbm],
         out_specs=(vmem, vmem),
@@ -576,6 +674,8 @@
             pltpu.VMEM((128, 4, 2048), BF),
             pltpu.VMEM((128, 4, 2048), BF),
             pltpu.VMEM((128, 4, 2048), BF),
+            pltpu.VMEM((16, 4, 2048), BF),
+            pltpu.VMEM((64, 128), BF),
             pltpu.VMEM((2048, 640), BF),
             pltpu.VMEM((128, 2048), BF),
             pltpu.VMEM((512, 640), F32),
@@ -596,7 +696,8 @@
             pltpu.VMEM((2, 16, 64, 2048), BF),
             pltpu.VMEM((512, 2048), F32),
             pltpu.VMEM((512, 128), F32),
-            dma((3,)), dma((8,)), dma((8,)), dma((8,)),
+            pltpu.VMEM((2, 2, 512, 128), BF),
+            dma((5,)), dma((8,)), dma((8,)), dma((8,)), dma((2, 2)), dma((2, 2)),
             dma((2, 8)), dma((2, 8)),
             dma((4,)), dma((4,)),
             dma((24,)), dma((16, 2)),

time: 64.5 us -> 59.8 us (0.927)
  the two profiles are of different devices: /device:TPU:33 before, /device:TPU:1 now
where the time goes in v2:
time: 59.8 us; the launch traced here: 59.7 us
  Pallas kernels  57.1 us (95%)
  local copies, waits for them, and re-layouts  1.94 us (3%)
  between operations  0.64 us (1%)
    pallas_call x1, Pallas kernels, layer(): pl.pallas_call(kernel, out_shape=(pltpu.VMEM((128, 4, 2048), BF), pltpu.V...  57.1 us
    unnamed x2, local copies, waits for them, and re-layouts  1.94 us

profile of v2, /device:TPU:1, one launch (start us, length us, event | category | flops | bytes accessed | tf_op | source)
XLA Modules:
  0.0 59.7 jit_solution(18024982431861399264)
XLA Ops:
  0.6 57.1 %mixer_layer.1 = (bf16[128,4,2048]{2,1,0:T(4,128)(2,1)S(1)}, f32[4,2,1024]{2,1,0:T(2,128)S(1)}) custom-call(bf16[1024,4,2048]{2,1,0:T(4,128)(2,1)} %x_hbm.1, f32[16,128]{1,0:T(8,128)} %bitcast.9, bf16[2048,128]{1,0:T(8,128)(2,1)} %pw.1, bf16[2048,128]{1,0:T(8,128)(2,1)} %gw.1, bf16[2048,128]{1,0:T(8,128)(2,1)} %qw.1, bf16[64,2048]{1,0:T(8,128)(2,1)} %bitcast.7, ...), custom_call_target="tpu_custom_call" | custom-call | tf_op jit(solution)/shard_map/mixer_layer/pallas_call | solution.py:665
  57.7 1.3 %copy.18 = bf16[128,4,2048]{2,1,0:T(4,128)(2,1)} copy(bf16[128,4,2048]{2,1,0:T(4,128)(2,1)S(1)} %get-tuple-element.6) | data formatting | bytes 4194304
  59.0 0.6 %copy.19 = f32[1024,4,2]{0,2,1:T(2,128)} copy(f32[1024,4,2]{0,2,1:T(2,128)S(1)} %bitcast.6) | data formatting | bytes 65536

commit v3 on v2

--- a/solution.py
+++ b/solution.py
@@ -18,6 +18,8 @@
 NSP = 16
 COMM = True
 NEAR = (0, 2)
+EARLY = {5: 1, 6: 3, 7: 2, 8: 4}
+OWN = 5
 FAR = (1, 3)
 
 
@@ -34,7 +36,7 @@
 def kernel(
     x_hbm, gain, pw, gw, qw, kw, vw, aw, mix, qg, kg, sink, outp, outa,
     out, lse,
-    xa, xc, xo, xe, edge, wb, kvt, pa, pc, tmp, inv, rsend, rbuf, qs, kvs, poolbuf, gate, agate, bias, band, ysend, yr, wg, acc, att, relay,
+    xb, xe, edge, rcol, wb, kvt, pa, pc, tmp, inv, rsend, rbuf, qs, kvs, poolbuf, gate, agate, bias, band, ysend, yr, wg, acc, att, relay,
     xsem, wsem, rs_send, rs_recv, lsend, lrecv, asend, arecv, hsend, hrecv, gsend, grecv, dsend, drecv,
 ):
     if COMM:
@@ -57,17 +59,13 @@
 
     def xcopy(k):
         return pltpu.make_async_copy(
-            x_hbm.at[pl.ds(order(k) * 128, 128)], (xa, xc)[k % 2], xsem.at[k % 2]
-        )
-
-    xown = pltpu.make_async_copy(x_hbm.at[pl.ds(tp * 128, 128)], xo, xsem.at[2])
-    xown.start()
+            x_hbm.at[pl.ds(order(k) * 128, 128)], xb.at[order(k)], xsem.at[k]
+        )
+
     xedge = (
-        pltpu.make_async_copy(x_hbm.at[pl.ds(0, 8)], xe.at[pl.ds(0, 8)], xsem.at[3]),
-        pltpu.make_async_copy(x_hbm.at[pl.ds(1016, 8)], xe.at[pl.ds(8, 8)], xsem.at[4]),
+        pltpu.make_async_copy(x_hbm.at[pl.ds(0, 8)], xe.at[pl.ds(0, 8)], xsem.at[8]),
+        pltpu.make_async_copy(x_hbm.at[pl.ds(1016, 8)], xe.at[pl.ds(8, 8)], xsem.at[9]),
     )
-    for cp in xedge:
-        cp.start()
 
     wcopies = [
         pltpu.make_async_copy(outp, wg.at[0, sp], wsem.at[0]),
@@ -79,10 +77,13 @@
         pltpu.make_async_copy(vw, kvt.at[pl.ds(64, 64)], wsem.at[6]),
         pltpu.make_async_copy(aw, wb.at[:, pl.ds(512, 128)], wsem.at[7]),
     ]
-    for cp in wcopies:
+    for cp in wcopies[:2]:
         cp.start()
-    xcopy(0).start()
-    xcopy(1).start()
+    xcopy(OWN).start()
+    for cp in wcopies[2:]:
+        cp.start()
+    for cp in xedge:
+        cp.start()
 
     zeros = jnp.zeros((64, 128), BF)
     poolbuf[0:64, :] = zeros
@@ -159,18 +160,10 @@
     def event0():
         send(0, 0, None, 1, 0)
         send(0, 0, None, -1, 0)
+
+    def event0_late():
         send(0, 0, None, 0, 1)
         send(0, 0, None, 0, -1)
-
-    def event1():
-        got(3, 0)
-        send(3, 0, 0, 1, 0)
-        got(1, 0)
-        send(1, 0, 1, -1, 0)
-        for da in (3, 1):
-            send(da, 0, None, 0, 1)
-            send(da, 0, None, 0, -1)
-            share(da, 0)
 
     def through(da):
         got(da, 3)
@@ -185,23 +178,33 @@
         got(da, 2, 1)
         share(da, 2)
 
+    def event1():
+        got(3, 0)
+        send(3, 0, 0, 1, 0)
+        got(1, 0)
+        send(1, 0, 1, -1, 0)
+        through(0)
+        for da in (3, 1):
+            send(da, 0, None, 0, 1)
+            send(da, 0, None, 0, -1)
+            share(da, 0)
+
     def event2():
         got(2, 0, 0)
         got(2, 0, 1)
         send(2, 0, None, 0, 1)
         send(2, 0, None, 0, -1)
         share(2, 0)
-        through(0)
 
     def event3():
         through(3)
         through(1)
-        far(0)
 
     def event4():
         through(2)
 
     def event5():
+        far(0)
         far(3)
         far(1)
 
@@ -213,7 +216,10 @@
     ones = jnp.ones((128, 128), BF)
     row128 = lax.broadcasted_iota(jnp.int32, (128, 128), 0)
     col128 = lax.broadcasted_iota(jnp.int32, (128, 128), 1)
-    head_ones = ((row128 // 64) == (col128 // 64)).astype(F32).astype(BF)
+    head_ones = (
+        (lax.broadcasted_iota(jnp.int32, (256, 256), 0) // 64)
+        == (lax.broadcasted_iota(jnp.int32, (256, 256), 1) // 64)
+    ).astype(F32).astype(BF)
 
     tpf = tp.astype(F32)
     s0 = sink[0]
@@ -265,8 +271,8 @@
             sq = sq + t * t
         return lax.rsqrt(split_dot(sq, ones) * (1.0 / 2048) + EPS)
 
-    xown.wait()
-    r = row_scale(xo[...].reshape(512, 2048))
+    xcopy(OWN).wait()
+    r = row_scale(xb[tp].reshape(512, 2048))
     packed = [
         jnp.sum(jnp.where(row128 == col128, r[128 * g : 128 * g + 128], 0.0), axis=0, keepdims=True)
         for g in range(4)
@@ -287,6 +293,9 @@
 
     for cp in wcopies[2:]:
         cp.wait()
+    for k in range(8):
+        if k != OWN:
+            xcopy(k).start()
 
     def prep(l, carry):
         rows = pl.ds(pl.multiple_of(l * 128, 128), 128)
@@ -333,10 +342,16 @@
         def _():
             halo_right()[1].start()
 
-    def multiply(k, lo, hi):
+    event0_late()
+
+    def multiply(k, lo, hi, at=None):
         p = (pa, pc)[k % 2]
-        x = (xa, xc)[k % 2][...].reshape(512, 2048)
-        p[:, lo:hi] = jnp.dot(x, wb[:, lo:hi], preferred_element_type=F32)
+        x = xb[order(k)].reshape(512, 2048)
+        at = lo if at is None else at
+        p[:, at : at + hi - lo] = jnp.dot(x, wb[:, lo:hi], preferred_element_type=F32)
+
+    def slot(k):
+        return 256 * ((k // 2) % 2)
 
     def ready(k):
         if COMM:
@@ -356,23 +371,29 @@
             axis=0,
         )
 
-    def finish_gates(k, r):
+    def finish_gates(k):
+        blk = order(k)
+        p = (pa, pc)[k % 2]
+        at = slot(k)
+        r = scales(k)
+        rcol[k] = r
+        rows = pl.ds(pl.multiple_of(blk * 512, 512), 512)
+        prows = pl.ds(pl.multiple_of(blk * 512 + 64, 64), 512)
+        poolbuf[prows, :] = (p[:, at : at + 128] * r).astype(BF)
+        gate[rows, :] = (p[:, at + 128 : at + 256] * r).astype(BF)
+
+    def finish_heads(k, r):
         blk = order(k)
         p = (pa, pc)[k % 2]
         rows = pl.ds(pl.multiple_of(blk * 512, 512), 512)
-        prows = pl.ds(pl.multiple_of(blk * 512 + 64, 64), 512)
-        poolbuf[prows, :] = (p[:, 0:128] * r).astype(BF)
-        gate[rows, :] = (p[:, 128:256] * r).astype(BF)
         agate[rows, :] = (p[:, 512:640] * r).astype(BF)
-
-    def finish_heads(k, r):
-        blk = order(k)
-        p = (pa, pc)[k % 2]
         q = (p[:, 256:384] * r).astype(BF).astype(F32)
-        rq = lax.rsqrt(split_dot(q * q, head_ones) * (1.0 / 64) + EPS)
+        kv = (p[:, 384:512] * r).astype(BF).astype(F32)
+        squares = jnp.concatenate([(q * q).astype(BF), (kv * kv).astype(BF)], axis=1)
+        means = jnp.dot(squares, head_ones, preferred_element_type=F32) * (1.0 / 64)
+        rq = lax.rsqrt(means[:, 0:128] + EPS)
+        rk = lax.rsqrt(means[:, 128:256] + EPS)
         tmp[0] = q * rq * qgain
-        kv = (p[:, 384:512] * r).astype(BF).astype(F32)
-        rk = lax.rsqrt(split_dot(kv * kv, head_ones) * (1.0 / 64) + EPS)
         tmp[1] = jnp.where(low, kv * rk * kgain, kv)
         for s in range(4):
             q = tmp[0, pl.ds(s, 128, stride=4), :]
@@ -461,67 +482,17 @@
         g = gate[pl.ds(start, 512), :].astype(F32)
         ysend[0, blk] = (mixed * silu(g)).astype(BF)
 
-    def step(k, top, pooling):
-        if top:
-            xcopy(k).wait()
-        if k > 0:
-            ready(k - 1)
-        if pooling:
-            pool_wait(order(k - 2))
-        if top:
-            multiply(k, 0, 256)
-        if k > 0:
-            r = scales(k - 1)
-            finish_gates(k - 1, r)
-        if top:
-            multiply(k, 256, 512)
-        if k > 0:
-            finish_heads(k - 1, r)
-        if top:
-            multiply(k, 512, 640)
-        if pooling:
-            pool(order(k - 2))
-        if top and k + 2 < 8:
-            xcopy(k + 2).start()
-        if k > 0:
-            edges(k - 1)
-        if pooling:
-            emit(0, order(k - 2))
-
-    for k in range(8):
-        step(k, True, k >= 3)
-        if k == 1:
-            event1()
-        if k == 3:
-            event2()
-        if k == 6:
-            event3()
-        if k == 5:
-            pass_on(0, c)
-        if k == 6:
-            pass_on(0, 1 - c)
-    step(8, False, True)
-
-    def pool_rest(k, carry):
-        blk = order(k % 8)
-        pool_wait(blk)
-        pool(blk)
-        emit(0, blk)
-        return carry
-
-    lax.fori_loop(7, 9, pool_rest, 0)
-    event4()
+    def att_wait(blk):
+        if COMM:
+            @pl.when((blk == 0) & (sp > 0))
+            def _():
+                halo_right()[0].wait_recv()
+
+            @pl.when((blk == 7) & (sp < NSP - 1))
+            def _():
+                halo_left()[0].wait_recv()
 
     def attend(blk):
-        if COMM:
-            @pl.when((blk == 0) & (sp > 0))
-            def _():
-                halo_right()[0].wait_recv()
-
-            @pl.when((blk == 7) & (sp < NSP - 1))
-            def _():
-                halo_left()[0].wait_recv()
-
         left = 3 * sp0 * (1 - (blk + 7) // 8)
         right = 2 + sp15 * ((blk + 1) // 8)
         for s in range(4):
@@ -546,24 +517,80 @@
             lse[s, :, pl.ds(pl.multiple_of(blk * 128, 128), 128)] = top + totals
         g = agate[pl.ds(pl.multiple_of(blk * 512, 512), 512), :].astype(F32)
         ysend[1, blk] = (att[...] * silu(g)).astype(BF)
+
+    def gate_step(j):
+        done = (2 * j - 2, 2 * j - 1) if j else ()
+        pools = {2: (1, 2), 3: (3, 4), 4: (5, 6)}.get(j, ())
+        for k in (2 * j, 2 * j + 1):
+            if k < 8 and k != OWN:
+                xcopy(k).wait()
+        for k in done:
+            ready(k)
+        for k in pools:
+            pool_wait(order(k))
+        for i in range(2):
+            if j < 4:
+                multiply(2 * j + i, 0, 256, slot(2 * j + i))
+            if done:
+                finish_gates(done[i])
+        for k in pools:
+            pool(order(k))
+        for k in pools:
+            emit(0, order(k))
+
+    def head_step(k):
+        late = (7, 0)[k] if k < 2 else None
+        if late is not None:
+            pool_wait(order(late))
+        if k in EARLY:
+            att_wait(order(EARLY[k]))
+        if k < 8:
+            multiply(k, 256, 512)
+        if k in EARLY:
+            attend(order(EARLY[k]))
+        if late is not None:
+            pool(order(late))
+        if k < 8:
+            multiply(k, 512, 640)
+        if k > 0:
+            finish_heads(k - 1, rcol[k - 1])
+            edges(k - 1)
+        if late is not None:
+            emit(0, order(late))
+        if k in EARLY:
+            emit(1, order(EARLY[k]))
+
+    for j in range(5):
+        gate_step(j)
+        if j == 2:
+            event1()
+    for k in range(9):
+        head_step(k)
+        if k == 0:
+            event2()
+            pass_on(0, c)
+        if k == 1:
+            pass_on(0, 1 - c)
+        if k == 4:
+            event3()
+        if k == 5:
+            event4()
+        if k == 7:
+            event5()
+        if k == 8:
+            pass_on(1, c)
+
+    def att_step(k, carry):
+        blk = order((7 + k + (k // 2) * 4) % 8)
+        att_wait(blk)
+        attend(blk)
         emit(1, blk)
-
-    def att_step(k, carry):
-        j = k // 2
-        d = (2 + 3 * j + 3 * (j // 2) + 2 * (j // 3)) % 4
-        d = (d + c * (4 - 2 * d)) % 4
-        attend(((chip + d) % 4) * 2 + (c + 1 + k) % 2)
-        if COMM:
-            for at, event in (
-                (3, event5),
-                (4, functools.partial(pass_on, 1, (c + 1) % 2)),
-                (5, event6),
-                (6, functools.partial(pass_on, 1, c)),
-            ):
+        if COMM:
+            for at, event in ((0, event6), (2, functools.partial(pass_on, 1, 1 - c))):
                 pl.when(k == at)(event)
         return carry
 
-    lax.fori_loop(0, 8, att_step, 0)
+    lax.fori_loop(0, 4, att_step, 0)
 
     def arrive(part, j):
         if COMM:
@@ -671,11 +698,10 @@
         in_specs=[hbm, vmem, hbm, hbm, hbm, hbm, hbm, hbm, vmem, vmem, vmem, smem, hbm, hbm],
         out_specs=(vmem, vmem),
         scratch_shapes=[
-            pltpu.VMEM((128, 4, 2048), BF),
-            pltpu.VMEM((128, 4, 2048), BF),
-            pltpu.VMEM((128, 4, 2048), BF),
+            pltpu.VMEM((8, 128, 4, 2048), BF),
             pltpu.VMEM((16, 4, 2048), BF),
             pltpu.VMEM((64, 128), BF),
+            pltpu.VMEM((8, 512, 128), F32),
             pltpu.VMEM((2048, 640), BF),
             pltpu.VMEM((128, 2048), BF),
             pltpu.VMEM((512, 640), F32),
@@ -697,7 +723,7 @@
             pltpu.VMEM((512, 2048), F32),
             pltpu.VMEM((512, 128), F32),
             pltpu.VMEM((2, 2, 512, 128), BF),
-            dma((5,)), dma((8,)), dma((8,)), dma((8,)), dma((2, 2)), dma((2, 2)),
+            dma((10,)), dma((8,)), dma((8,)), dma((8,)), dma((2, 2)), dma((2, 2)),
             dma((2, 8)), dma((2, 8)),
             dma((4,)), dma((4,)),
             dma((24,)), dma((16, 2)),

time: 59.8 us -> 55.2 us (0.923)
  the two profiles are of different devices: /device:TPU:1 before, /device:TPU:33 now
where the time goes in v3:
time: 55.2 us; the launch traced here: 55 us
  Pallas kernels  52.4 us (95%)
  local copies, waits for them, and re-layouts  1.94 us (4%)
  between operations  0.64 us (1%)
    pallas_call x1, Pallas kernels, layer(): pl.pallas_call(kernel, out_shape=(pltpu.VMEM((128, 4, 2048), BF), pltpu.V...  52.4 us
    unnamed x2, local copies, waits for them, and re-layouts  1.94 us

profile of v3, /device:TPU:33, one launch (start us, length us, event | category | flops | bytes accessed | tf_op | source)
XLA Modules:
  0.0 55.0 jit_solution(893962300777466604)
XLA Ops:
  0.6 52.4 %mixer_layer.1 = (bf16[128,4,2048]{2,1,0:T(4,128)(2,1)S(1)}, f32[4,2,1024]{2,1,0:T(2,128)S(1)}) custom-call(bf16[1024,4,2048]{2,1,0:T(4,128)(2,1)} %x_hbm.1, f32[16,128]{1,0:T(8,128)} %bitcast.9, bf16[2048,128]{1,0:T(8,128)(2,1)} %pw.1, bf16[2048,128]{1,0:T(8,128)(2,1)} %gw.1, bf16[2048,128]{1,0:T(8,128)(2,1)} %qw.1, bf16[64,2048]{1,0:T(8,128)(2,1)} %bitcast.7, ...), custom_call_target="tpu_custom_call" | custom-call | tf_op jit(solution)/shard_map/mixer_layer/pallas_call | solution.py:692
  53.1 1.3 %copy.18 = bf16[128,4,2048]{2,1,0:T(4,128)(2,1)} copy(bf16[128,4,2048]{2,1,0:T(4,128)(2,1)S(1)} %get-tuple-element.6) | data formatting | bytes 4194304
  54.4 0.6 %copy.19 = f32[1024,4,2]{0,2,1:T(2,128)} copy(f32[1024,4,2]{0,2,1:T(2,128)S(1)} %bitcast.6) | data formatting | bytes 65536

commit v4 on v3

--- a/solution.py
+++ b/solution.py
@@ -566,14 +566,14 @@
             event1()
     for k in range(9):
         head_step(k)
-        if k == 0:
+        if k == 1:
             event2()
             pass_on(0, c)
-        if k == 1:
+        if k == 2:
             pass_on(0, 1 - c)
         if k == 4:
             event3()
-        if k == 5:
+        if k == 6:
             event4()
         if k == 7:
             event5()
@@ -623,7 +623,7 @@
         )
         return carry
 
-    lax.fori_loop(0, 4, out_pool_step, 0)
+    lax.fori_loop(0, 4, out_pool_step, 0, unroll=True)
 
     def attn_part(cols, d):
         src = [(chip + e) % 4 for e in d]
@@ -644,11 +644,11 @@
     for d in NEAR:
         for h in range(2):
             arrive(1, 2 * ((chip + d) % 4) + h)
-    lax.fori_loop(0, 4, out_near_step, 0)
+    lax.fori_loop(0, 4, out_near_step, 0, unroll=True)
     for d in FAR:
         for h in range(2):
             arrive(1, 2 * ((chip + d) % 4) + h)
-    lax.fori_loop(0, 4, out_attn_step, 0)
+    lax.fori_loop(0, 4, out_attn_step, 0, unroll=True)
 
     if COMM:
         for part in range(2):

time: 55.2 us -> 53.4 us (0.967)
  the two profiles are of different devices: /device:TPU:33 before, /device:TPU:7 now
where the time goes in v4:
time: 53.4 us; the launch traced here: 53.2 us
  Pallas kernels  50.6 us (95%)
  local copies, waits for them, and re-layouts  1.94 us (4%)
  between operations  0.64 us (1%)
    pallas_call x1, Pallas kernels, layer(): pl.pallas_call(kernel, out_shape=(pltpu.VMEM((128, 4, 2048), BF), pltpu.V...  50.6 us
    unnamed x2, local copies, waits for them, and re-layouts  1.94 us

profile of v4, /device:TPU:7, one launch (start us, length us, event | category | flops | bytes accessed | tf_op | source)
XLA Modules:
  0.0 53.2 jit_solution(9897184250951914113)
XLA Ops:
  0.6 50.6 %mixer_layer.1 = (bf16[128,4,2048]{2,1,0:T(4,128)(2,1)S(1)}, f32[4,2,1024]{2,1,0:T(2,128)S(1)}) custom-call(bf16[1024,4,2048]{2,1,0:T(4,128)(2,1)} %x_hbm.1, f32[16,128]{1,0:T(8,128)} %bitcast.9, bf16[2048,128]{1,0:T(8,128)(2,1)} %pw.1, bf16[2048,128]{1,0:T(8,128)(2,1)} %gw.1, bf16[2048,128]{1,0:T(8,128)(2,1)} %qw.1, bf16[64,2048]{1,0:T(8,128)(2,1)} %bitcast.7, ...), custom_call_target="tpu_custom_call" | custom-call | tf_op jit(solution)/shard_map/mixer_layer/pallas_call | solution.py:692
  51.3 1.3 %copy.18 = bf16[128,4,2048]{2,1,0:T(4,128)(2,1)} copy(bf16[128,4,2048]{2,1,0:T(4,128)(2,1)S(1)} %get-tuple-element.6) | data formatting | bytes 4194304
  52.6 0.6 %copy.19 = f32[1024,4,2]{0,2,1:T(2,128)} copy(f32[1024,4,2]{0,2,1:T(2,128)S(1)} %bitcast.6) | data formatting | bytes 65536
